TPU v7x, 32 devices: a whole 2x2x4 slice. The times are simulated.
32 devices in a mesh: ep: 8 (over z, x), tp: 4 (over y, core).
Axes of the slice: x: 2, y: 2, z: 4, core: 2. Of those that a mesh axis runs over, the one named last changes fastest.
Arguments:
- tokens: bfloat16 [32, 2048], P('ep'), may hold values from -6 to 6
- norm_gain: bfloat16 [2048], replicated, may hold values from 0.099609375 to 1.8984375
- in_weight: bfloat16 [2048, 1024], P(None, 'tp'), may hold values from -0.125 to 0.125
- decay_rate: float32 [64, 64], P('tp'), may hold values from 0.05 to 1
- frequency: float32 [64, 64], P('tp'), may hold values from -3 to 3
- log_step: float32 [64], P('tp'), may hold values from -2.3 to 0.7
- input_real: float32 [64, 64, 16], P('tp'), may hold values from -1.75 to 1.75
- input_imag: float32 [64, 64, 16], P('tp'), may hold values from -1.75 to 1.75
- output_real: float32 [64, 16, 64], P('tp'), may hold values from -0.5 to 0.5
- output_imag: float32 [64, 16, 64], P('tp'), may hold values from -0.5 to 0.5
- skip_gain: float32 [1024], P('tp'), may hold values from -3 to 3
- state_real: float32 [32, 64, 64], P('ep', 'tp'), may hold values from -6 to 6
- state_imag: float32 [32, 64, 64], P('ep', 'tp'), may hold values from -6 to 6
- out_weight: bfloat16 [1024, 2048], P('tp'), may hold values from -0.1875 to 0.1875
- ffn_gain: bfloat16 [2048], replicated, may hold values from 0.099609375 to 1.8984375
- expert_ids: int32 [32, 2], replicated, may hold values from 0 to 7, all different within a row; in each aligned block of 4 rows (0 to 3, 4 to 7, ...) at most 2 rows name the same one
- route_weights: float32 [32, 2], P('ep'), may hold values from 0.2 to 1
- gate_weight: bfloat16 [2048, 65536], P(None, ('ep', 'tp')), may hold values from -0.125 to 0.125
- up_weight: bfloat16 [2048, 65536], P(None, ('ep', 'tp')), may hold values from -0.125 to 0.125
- down_weight: bfloat16 [65536, 2048], P('ep', 'tp'), may hold values from -0.0625 to 0.0625
Outputs:
- mixed: bfloat16 [32, 2048], P('ep', 'tp')
- new_real: float32 [32, 64, 64], P('ep', 'tp')
- new_imag: float32 [32, 64, 64], P('ep', 'tp')
Inputs may be any that keep to these rules, and one draw needn't show every extreme that they name: `expert_ids`: the 2 experts of a row differ. In each aligned block of 4 rows (the rows of one index of ep) no expert is named by more than 2 rows, and in some blocks one expert is named by exactly 2 rows.
All inputs are finite; a program needn't handle non-finite values.
Results may differ from a plain program's by a relative error of at most 0.007.
Values may be sent and summed in bfloat16 or wider, within the bound.
A program may use at most 64 MiB of HBM per device.

v0:
```python
import jax
import jax.numpy as jnp
from jax import lax
from jax.sharding import PartitionSpec as P

EXPERTS = 8
EPSILON = 1e-06


def rms_scale(values, gain):
    floats = values.astype(jnp.float32)
    return (
        floats
        * lax.rsqrt(jnp.mean(floats * floats, axis=-1, keepdims=True) + EPSILON)
        * gain.astype(jnp.float32)
    )


def discretize(decay_rate, frequency, log_step, input_real, input_imag):
    step_size = jnp.exp(log_step)[:, None]
    lam_real = -decay_rate
    magnitude = jnp.exp(lam_real * step_size)
    turned = frequency * step_size
    bar_real = magnitude * jnp.cos(turned)
    bar_imag = magnitude * jnp.sin(turned)
    denom = lam_real * lam_real + frequency * frequency
    minus_one = bar_real - 1.0
    factor_real = (minus_one * lam_real + bar_imag * frequency) / denom
    factor_imag = (bar_imag * lam_real - minus_one * frequency) / denom
    b_real = factor_real[..., None] * input_real - factor_imag[..., None] * input_imag
    b_imag = factor_real[..., None] * input_imag + factor_imag[..., None] * input_real
    return (bar_real, bar_imag, b_real, b_imag)


def state_update(
    projected,
    state_real,
    state_imag,
    decay_rate,
    frequency,
    log_step,
    input_real,
    input_imag,
    output_real,
    output_imag,
    skip_gain,
):
    bar_real, bar_imag, b_real, b_imag = discretize(
        decay_rate, frequency, log_step, input_real, input_imag
    )
    count, groups, _ = state_real.shape
    high = lax.Precision.HIGHEST
    grouped = projected.astype(jnp.float32).reshape(count, groups, -1)
    drive_real = jnp.einsum("sgp,gnp->sgn", grouped, b_real, precision=high)
    drive_imag = jnp.einsum("sgp,gnp->sgn", grouped, b_imag, precision=high)
    new_real = bar_real * state_real - bar_imag * state_imag + drive_real
    new_imag = bar_real * state_imag + bar_imag * state_real + drive_imag
    readout = jnp.einsum("sgn,gpn->sgp", new_real, output_real, precision=high) - jnp.einsum(
        "sgn,gpn->sgp", new_imag, output_imag, precision=high
    )
    readout = readout.reshape(count, -1) + skip_gain * grouped.reshape(count, -1)
    return (jax.nn.gelu(readout).astype(jnp.bfloat16), new_real, new_imag)


def slot_table(own_ids, own_weights, slot_count):
    expert_range = jnp.arange(EXPERTS, dtype=jnp.int32)
    onehot = (own_ids[:, :, None] == expert_range).astype(jnp.int32)
    flat = onehot.reshape(-1, EXPERTS)
    before = (jnp.cumsum(flat, axis=0) - flat).reshape(onehot.shape)
    slots = jnp.arange(slot_count, dtype=jnp.int32)
    match = (before[..., None] == slots) & (onehot[..., None] > 0)
    table = jnp.sum(jnp.where(match, own_weights[:, :, None, None], 0.0), axis=1)
    return jnp.transpose(table, (1, 2, 0))


def shards(
    tokens,
    norm_gain,
    in_weight,
    decay_rate,
    frequency,
    log_step,
    input_real,
    input_imag,
    output_real,
    output_imag,
    skip_gain,
    state_real,
    state_imag,
    out_weight,
    ffn_gain,
    expert_ids,
    route_weights,
    gate_weight,
    up_weight,
    down_weight,
):
    normed_in = rms_scale(tokens, norm_gain).astype(jnp.bfloat16)
    projected = jnp.dot(normed_in, in_weight, preferred_element_type=jnp.float32).astype(
        jnp.bfloat16
    )
    activated, new_real, new_imag = state_update(
        projected,
        state_real,
        state_imag,
        decay_rate,
        frequency,
        log_step,
        input_real,
        input_imag,
        output_real,
        output_imag,
        skip_gain,
    )
    delta = lax.psum(jnp.dot(activated, out_weight, preferred_element_type=jnp.float32), "tp")
    hidden_state = (tokens.astype(jnp.float32) + delta).astype(jnp.bfloat16)
    normed = rms_scale(hidden_state, ffn_gain).astype(jnp.bfloat16)
    seq_count, width = normed.shape
    slot_count = seq_count // 2
    group_span = lax.axis_size("ep") // EXPERTS
    my_index = lax.axis_index("ep")
    own_ids = lax.dynamic_slice_in_dim(expert_ids, my_index * seq_count, seq_count, 0)
    unit_weights = jnp.ones(own_ids.shape, jnp.float32)
    select = slot_table(own_ids, unit_weights, slot_count)
    outgoing = jnp.einsum(
        "xcs,sd->xcd", select.astype(jnp.bfloat16), normed, preferred_element_type=jnp.float32
    ).astype(jnp.bfloat16)
    received = lax.all_to_all(
        jnp.repeat(outgoing, group_span, axis=0), "ep", split_axis=0, concat_axis=0, tiled=True
    )
    slot_rows = received.reshape(-1, width)
    gate_pre = jnp.dot(slot_rows, gate_weight, preferred_element_type=jnp.float32)
    up_pre = jnp.dot(slot_rows, up_weight, preferred_element_type=jnp.float32)
    hidden = (jax.nn.silu(gate_pre) * up_pre).astype(jnp.bfloat16)
    quarter = down_weight.shape[1]
    partial_out = jnp.dot(
        lax.all_gather(hidden, "tp", axis=1, tiled=True),
        down_weight,
        preferred_element_type=jnp.float32,
    )
    rounded = partial_out.astype(jnp.bfloat16).reshape(-1, slot_count, quarter)
    returned = lax.all_to_all(rounded, "ep", split_axis=0, concat_axis=0, tiled=True)
    summed = (
        returned.astype(jnp.float32).reshape(EXPERTS, group_span, slot_count, quarter).sum(axis=1)
    )
    weight_table = slot_table(own_ids, route_weights, slot_count)
    routed = jnp.einsum("xcs,xcd->sd", weight_table, summed, precision=lax.Precision.HIGHEST)
    residual = lax.dynamic_slice_in_dim(hidden_state, lax.axis_index("tp") * quarter, quarter, 1)
    mixed = (residual.astype(jnp.float32) + routed).astype(jnp.bfloat16)
    return (mixed, new_real, new_imag)


def solution(mesh):
    in_specs = (
        P("ep", None),
        P(),
        P(None, "tp"),
        P("tp", None),
        P("tp", None),
        P("tp"),
        P("tp", None, None),
        P("tp", None, None),
        P("tp", None, None),
        P("tp", None, None),
        P("tp"),
        P("ep", "tp", None),
        P("ep", "tp", None),
        P("tp", None),
        P(),
        P(),
        P("ep", None),
        P(None, ("ep", "tp")),
        P(None, ("ep", "tp")),
        P("ep", "tp"),
    )
    out_specs = (P("ep", "tp"), P("ep", "tp", None), P("ep", "tp", None))
    return jax.shard_map(shards, mesh=mesh, in_specs=in_specs, out_specs=out_specs, check_vma=False)
```

profile of v0, /device:TPU:0, one launch (start us, length us, event | category | flops | bytes accessed | tf_op | source)
XLA Modules:
  0.0 71.3 jit_solution(13652618909060821899)
XLA Ops:
  0.6 0.0 copy-start
  0.7 0.8 %constant_dynamic-slice_fusion = s32[4,2]{0,1:T(2,128)S(1)} fusion(s32[32,2]{0,1:T(2,128)} %param.35, s32[]{:T(128)S(6)} %select_n.14), kind=kLoop, calls=%fused_computation.78 | loop fusion | bytes 68 | tf_op jit(solution)/shard_map/dynamic_slice | solution.py:122
  1.5 0.1 copy.71
  1.6 0.1 eq.56
  1.7 0.1 fusion.42
  1.7 0.7 exp.10
  2.4 0.9 %fusion.19 = f32[4]{0:T(128)S(1)} fusion(bf16[4,2048]{1,0:T(4,128)(2,1)} %param.20), kind=kLoop, calls=%fused_computation.32 | loop fusion | flops 24572 | bytes 16400 | tf_op jit(solution)/shard_map/reduce_sum | solution.py:14
  3.3 0.7 convert_element_type.68
  4.0 1.5 %convolution_convert_fusion.2 = bf16[4,256]{1,0:T(4,128)(2,1)S(1)} fusion(bf16[2048,256]{1,0:T(8,128)(2,1)} %param.22, bf16[4,2048]{1,0:T(4,128)(2,1)} %param.20, f32[2048]{0:T(1024)S(1)} %convert_element_type.68, f32[4]{0:T(128)S(1)} %add_rsqrt_fusion.1), kind=kOutput, calls=%fused_computation.13 | convolution fusion | flops 4228096 | bytes 1075216 | tf_op jit(solution)/shard_map/dot_general | solution.py:99
  5.5 0.1 reshape.72
  5.6 0.8 %cosine_multiply_fusion = (f32[16,64]{1,0:T(8,128)S(1)}, f32[16,64]{1,0:T(8,128)S(1)}, f32[16,64]{1,0:T(8,128)S(1)}, f32[16,64]{1,0:T(8,128)S(1)}) fusion(f32[16,64]{1,0:T(8,128)} %param.24, f32[16,64]{1,0:T(8,128)} %param.23, f32[16]{0:T(128)S(1)} %exp.10), kind=kLoop, calls=%fused_computation.51 | loop fusion | flops 17408 | bytes 24640 | tf_op jit(solution)/shard_map/mul | solution.py:24
  6.4 1.2 %fusion.2 = f32[4,16,64]{2,0,1:T(4,128)S(1)} fusion(f32[16,64,16]{1,2,0:T(8,128)} %param.26, f32[16,64,16]{1,2,0:T(8,128)} %param.27, f32[16,64]{1,0:T(8,128)S(1)} %get-tuple-element.21, f32[16,64]{1,0:T(8,128)S(1)} %get-tuple-element.20, f32[4,16,64]{2,1,0:T(8,128)} %param.32, f32[4,16,64]{2,1,0:T(8,128)} %param.31, f32[16,64]{1,0:T(8,128)S(1)} %get-tuple-element.22, ...), kind=kOutput, calls=%fused_computation.6 | convolution fusion | flops 851968 | bytes 198656 | tf_op jit(solution)/shard_map/sgp,gnp->sgn/dot_general | solution.py:55
  7.6 1.2 %fusion.3 = f32[4,16,64]{2,0,1:T(4,128)S(1)} fusion(f32[16,64,16]{1,2,0:T(8,128)} %param.27, f32[16,64,16]{1,2,0:T(8,128)} %param.26, f32[16,64]{1,0:T(8,128)S(1)} %get-tuple-element.21, f32[16,64]{1,0:T(8,128)S(1)} %get-tuple-element.20, f32[4,16,64]{2,1,0:T(8,128)} %param.32, f32[4,16,64]{2,1,0:T(8,128)} %param.31, f32[16,64]{1,0:T(8,128)S(1)} %get-tuple-element.22, ...), kind=kOutput, calls=%fused_computation.8 | convolution fusion | flops 851968 | bytes 198656 | tf_op jit(solution)/shard_map/sgp,gnp->sgn/dot_general | solution.py:54
  8.8 0.1 fusion.45
  8.9 0.1 fusion.43
  9.0 0.7 convert_element_type.80
  9.7 1.2 %fusion.60 = f32[16,4,16]{2,1,0:T(4,128)S(1)} fusion(f32[4,16,64]{2,0,1:T(4,128)S(1)} %fusion.3, f32[16,16,64]{2,1,0:T(8,128)} %param.28), kind=kOutput, calls=%fused_computation.84 | convolution fusion | flops 786432 | bytes 86016 | tf_op jit(solution)/shard_map/sgn,gpn->sgp/dot_general | solution.py:58
  10.9 1.2 %fusion.1 = f32[4,16,16]{2,0,1:T(4,128)S(1)} fusion(f32[16,4,16]{2,1,0:T(4,128)S(1)} %fusion.60, f32[4,16,64]{2,0,1:T(4,128)S(1)} %fusion.2, f32[16,16,64]{2,1,0:T(8,128)} %param.29), kind=kOutput, calls=%fused_computation.4 | convolution fusion | flops 787456 | bytes 90112 | tf_op jit(solution)/shard_map/sgn,gpn->sgp/dot_general | solution.py:58
  12.1 0.1 reshape.73
  12.2 0.0 copy-done
  12.2 0.9 %fusion.46 = f32[4,2048]{1,0:T(4,128)S(1)} fusion(bf16[256,2048]{1,0:T(8,128)(2,1)S(1)} %copy-done, f32[4,256]{1,0:T(4,128)S(1)} %reshape.73, bf16[4,256]{1,0:T(4,128)(2,1)S(1)} %convolution_convert_fusion.2, f32[256]{0:T(256)} %param.30), kind=kOutput, calls=%fused_computation.69 | convolution fusion | flops 4206592 | bytes 1088512 | tf_op jit(solution)/shard_map/dot_general | solution.py:115
  13.2 12.9 %psum.7 = f32[4,2048]{1,0:T(4,128)S(1)} all-reduce(f32[4,2048]{1,0:T(4,128)S(1)} %fusion.46), channel_id=1, replica_groups=mesh['ep'=8,'tp'=4] {'tp'}, use_global_device_ids=true, to_apply=%region_1.0 | all-reduce | flops 8192 | bytes 65536 | tf_op jit(solution)/shard_map/psum | solution.py:115
  26.1 0.9 %fusion.16 = (f32[4]{0:T(128)S(1)}, bf16[4,2048]{1,0:T(4,128)(2,1)S(1)}) fusion(f32[4,2048]{1,0:T(4,128)S(1)} %psum.7, bf16[4,2048]{1,0:T(4,128)(2,1)} %param.20), kind=kLoop, calls=%fused_computation.29 | loop fusion | flops 49148 | bytes 65552 | tf_op jit(solution)/shard_map/reduce_sum | solution.py:14
  26.9 0.8 %select_reduce_fusion.1 = (f32[4,8,2]{1,0,2:T(4,128)S(1)}, bf16[4,8,2]{1,0,2:T(4,128)(2,1)S(1)}) fusion(f32[4,2]{0,1:T(2,128)} %param.36, s32[4,2,8]{2,0,1:T(4,128)S(1)} %copy.73, pred[4,2,8]{2,0,1:T(4,128)(4,1)S(1)} %copy.74), kind=kLoop, calls=%fused_computation.45 | loop fusion | flops 640 | bytes 736 | tf_op jit(solution)/shard_map/reduce_sum | solution.py:72
  27.7 0.2 convolution_convert_fusion
  27.9 0.1 copy.75
  28.0 12.5 %all_to_all.10 = bf16[8,2,2048]{2,1,0:T(2,128)(2,1)S(1)} all-to-all(bf16[8,2,2048]{2,1,0:T(2,128)(2,1)S(1)} %copy.75), channel_id=1, replica_groups=mesh['ep'=8,'tp'=4] {'ep'}, dimensions={0} | all-to-all | bytes 131072 | tf_op jit(solution)/shard_map/all_to_all | solution.py:128
  40.5 4.6 %fusion.61 = f32[16,2048]{1,0:T(8,128)S(1)} fusion(bf16[16,2048]{1,0:T(8,128)(2,1)S(1)} %reshape.74, bf16[2048,2048]{1,0:T(8,128)(2,1)} %param.37), kind=kOutput, calls=%fused_computation.85 | convolution fusion | flops 134217728 | bytes 8585216 | tf_op jit(solution)/shard_map/dot_general | solution.py:132
  45.1 4.6 %fusion = bf16[16,2048]{1,0:T(8,128)(2,1)S(1)} fusion(bf16[16,2048]{1,0:T(8,128)(2,1)S(1)} %reshape.74, bf16[2048,2048]{1,0:T(8,128)(2,1)} %param.38, f32[16,2048]{1,0:T(8,128)S(1)} %fusion.61), kind=kOutput, calls=%fused_computation.2 | convolution fusion | flops 134414336 | bytes 8650752 | tf_op jit(solution)/shard_map/dot_general | solution.py:133
  49.7 5.8 %all_gather.3 = bf16[16,8192]{1,0:T(8,128)(2,1)S(1)} all-gather(bf16[16,2048]{1,0:T(8,128)(2,1)S(1)} %fusion), channel_id=1, replica_groups=mesh['ep'=8,'tp'=4] {'tp'}, dimensions={1}, use_global_device_ids=true | all-gather | bytes 327680 | tf_op jit(solution)/shard_map/all_gather | solution.py:137
  55.5 4.6 %convolution_convert_fusion.1 = bf16[16,512]{1,0:T(8,128)(2,1)S(1)} fusion(bf16[16,8192]{1,0:T(8,128)(2,1)S(1)} %all_gather.3, bf16[8192,512]{1,0:T(8,128)(2,1)} %param.39), kind=kOutput, calls=%fused_computation.9 | convolution fusion | flops 134225920 | bytes 8667136 | tf_op jit(solution)/shard_map/dot_general | solution.py:136
  60.0 0.6 reshape.75
  60.7 3.3 %all-to-all-start.1 = ((bf16[8,2,512]{2,1,0:T(2,128)(2,1)}), bf16[8,2,512]{2,1,0:T(2,128)(2,1)S(1)}, u32[]{:S(2)}, u32[]{:S(2)}) async-start(bf16[8,2,512]{2,1,0:T(2,128)(2,1)} %reshape.75), calls=%async_computation.1 | async-start | bytes 32768 | tf_op jit(solution)/shard_map/all_to_all | solution.py:142
  64.0 0.6 copy.77
  64.6 0.6 copy.78
  65.2 5.3 %all-to-all-done.1 = bf16[8,2,512]{2,1,0:T(2,128)(2,1)S(1)} async-done(((bf16[8,2,512]{2,1,0:T(2,128)(2,1)}), bf16[8,2,512]{2,1,0:T(2,128)(2,1)S(1)}, u32[]{:S(2)}, u32[]{:S(2)}) %all-to-all-start.1) | async-done | bytes 16416 | tf_op jit(solution)/shard_map/all_to_all | solution.py:142
  70.5 0.8 %fusion.5 = bf16[4,512]{1,0:T(4,128)(2,1)} fusion(bf16[8,2,512]{2,1,0:T(2,128)(2,1)S(1)} %all-to-all-done.1, f32[4,8,2]{1,0,2:T(4,128)S(1)} %get-tuple-element.15, bf16[4,2048]{1,0:T(4,128)(2,1)S(1)} %get-tuple-element.18, s32[]{:T(128)S(6)} %select_n.13), kind=kOutput, calls=%fused_computation.12 | convolution fusion | flops 399360 | bytes 24836 | tf_op jit(solution)/shard_map/xcs,xcd->sd/dot_general | solution.py:147
  (7 shorter events, 0.1 us)
Async XLA Ops:
  0.6 11.6 %copy-start = (bf16[256,2048]{1,0:T(8,128)(2,1)S(1)}, bf16[256,2048]{1,0:T(8,128)(2,1)}, u32[]{:S(2)}) copy-start(bf16[256,2048]{1,0:T(8,128)(2,1)} %param.33) | copy-start | bytes 3145732
  60.7 9.9 %all-to-all-start.1 = ((bf16[8,2,512]{2,1,0:T(2,128)(2,1)}), bf16[8,2,512]{2,1,0:T(2,128)(2,1)S(1)}, u32[]{:S(2)}, u32[]{:S(2)}) async-start(bf16[8,2,512]{2,1,0:T(2,128)(2,1)} %reshape.75), calls=%async_computation.1 | async-start | bytes 32768 | tf_op jit(solution)/shard_map/all_to_all | solution.py:142
where the time goes:
time: 72.1 us; the launch traced here: 71.3 us
  blocking collectives  31.2 us (43%)
  matrix products  22 us (31%)
  waiting for transfers between devices  5.28 us (7%)
  other arithmetic  4.97 us (7%)
  local copies, waits for them, and re-layouts  3.84 us (5%)
  starting transfers between devices  3.33 us (5%)
  between operations  0.73 us (1%)
    psum x1, blocking collectives, shards(): lax.psum(jnp.dot(activated, out_weight, preferred_element_type=jnp.float3...  12.9 us
    all_to_all x1, blocking collectives, shards(): lax.all_to_all(jnp.repeat(outgoing, group_span, axis=0), 'ep', split_axis...  12.5 us
    all_gather x1, blocking collectives, shards(): lax.all_gather(hidden, 'tp', axis=1, tiled=True)  5.77 us
    all_to_all x1, waiting for transfers between devices, shards(): lax.all_to_all(rounded, 'ep', split_axis=0, concat_axis=0, tiled=True)  5.28 us
    dot_general x1, matrix products, shards(): up_pre = jnp.dot(slot_rows, up_weight, preferred_element_type=jnp.float32)  4.58 us
    dot_general x1, matrix products, shards(): jnp.dot(slot_rows, gate_weight, preferred_element_type=jnp.float32)  4.58 us
    dot_general x1, matrix products, shards(): jnp.dot(lax.all_gather(hidden, 'tp', axis=1, tiled=True), down_weight, pr...  4.56 us
    all_to_all x1, starting transfers between devices, shards(): lax.all_to_all(rounded, 'ep', split_axis=0, concat_axis=0, tiled=True)  3.33 us
  transfers between devices with their start and end apart: 1, of which 1 were waited for; matrix products, arithmetic and copies ran while one was open for 2% of the time, Pallas kernels for 0%

commit v1 on v0

--- a/solution.py
+++ b/solution.py
@@ -134,7 +134,7 @@
     hidden = (jax.nn.silu(gate_pre) * up_pre).astype(jnp.bfloat16)
     quarter = down_weight.shape[1]
     partial_out = jnp.dot(
-        lax.all_gather(hidden, "tp", axis=1, tiled=True),
+        jnp.concatenate(lax.all_gather(hidden, "tp"), axis=1),
         down_weight,
         preferred_element_type=jnp.float32,
     )

time: 72.1 us -> 67 us (0.929)
  matrix products: 22 us -> 15.4 us
  local copies, waits for them, and re-layouts: 3.84 us -> 5.23 us
    dot_general x1, matrix products: 4.58 us -> 1.2 us  [shards(): up_pre = jnp.dot(slot_rows, up_weight, preferred_element_type=jnp.float32)]
    dot_general x1, matrix products: 4.56 us -> 1.18 us  [shards(): jnp.dot(jnp.concatenate(lax.all_gather(hidden, 'tp'), axis=1), down_weigh...]
    unnamed x4 -> x11, local copies, waits for them, and re-layouts: 1.24 us -> 2.43 us
where the time goes in v1:
time: 67 us; the launch traced here: 66.3 us
  blocking collectives  31.3 us (47%)
  matrix products  15.4 us (23%)
  waiting for transfers between devices  5.28 us (8%)
  local copies, waits for them, and re-layouts  5.23 us (8%)
  other arithmetic  4.97 us (7%)
  starting transfers between devices  3.33 us (5%)
  between operations  0.78 us (1%)
    psum x1, blocking collectives, shards(): lax.psum(jnp.dot(activated, out_weight, preferred_element_type=jnp.float3...  12.9 us
    all_to_all x1, blocking collectives, shards(): lax.all_to_all(jnp.repeat(outgoing, group_span, axis=0), 'ep', split_axis...  12.5 us
    all_gather x1, blocking collectives, shards(): lax.all_gather(hidden, 'tp')  5.9 us
    all_to_all x1, waiting for transfers between devices, shards(): lax.all_to_all(rounded, 'ep', split_axis=0, concat_axis=0, tiled=True)  5.28 us
    dot_general x1, matrix products, shards(): jnp.dot(slot_rows, gate_weight, preferred_element_type=jnp.float32)  4.73 us
    all_to_all x1, starting transfers between devices, shards(): lax.all_to_all(rounded, 'ep', split_axis=0, concat_axis=0, tiled=True)  3.33 us
    unnamed x11, local copies, waits for them, and re-layouts  2.43 us
    reduce_sum x2, other arithmetic, rms_scale(): jnp.mean(floats * floats, axis=-1, keepdims=True) + EPSILON  1.7 us
  transfers between devices with their start and end apart: 1, of which 1 were waited for; matrix products, arithmetic and copies ran while one was open for 2% of the time, Pallas kernels for 0%

profile of v1, /device:TPU:0, one launch (start us, length us, event | category | flops | bytes accessed | tf_op | source)
XLA Modules:
  0.0 66.3 jit_solution(18267123518737041214)
XLA Ops:
  0.6 0.0 copy-start
  0.7 0.8 %constant_dynamic-slice_fusion = s32[4,2]{0,1:T(2,128)S(1)} fusion(s32[32,2]{0,1:T(2,128)} %param.35, s32[]{:T(128)S(6)} %select_n.14), kind=kLoop, calls=%fused_computation.78 | loop fusion | bytes 68 | tf_op jit(solution)/shard_map/dynamic_slice | solution.py:122
  1.5 0.1 copy.73
  1.6 0.1 eq.56
  1.7 0.1 fusion.42
  1.7 0.7 exp.10
  2.4 0.9 %fusion.19 = f32[4]{0:T(128)S(1)} fusion(bf16[4,2048]{1,0:T(4,128)(2,1)} %param.20), kind=kLoop, calls=%fused_computation.32 | loop fusion | flops 24572 | bytes 16400 | tf_op jit(solution)/shard_map/reduce_sum | solution.py:14
  3.3 0.7 %convert_element_type.68 = f32[2048]{0:T(1024)S(1)} convert(bf16[2048]{0:T(1024)(128)(2,1)} %param.21) | non-fusion elementwise | flops 2048 | bytes 12288 | tf_op jit(solution)/shard_map/convert_element_type | solution.py:15
  4.0 1.5 %convolution_convert_fusion.2 = bf16[4,256]{1,0:T(4,128)(2,1)S(1)} fusion(bf16[2048,256]{1,0:T(8,128)(2,1)} %param.22, bf16[4,2048]{1,0:T(4,128)(2,1)} %param.20, f32[2048]{0:T(1024)S(1)} %convert_element_type.68, f32[4]{0:T(128)S(1)} %add_rsqrt_fusion.1), kind=kOutput, calls=%fused_computation.13 | convolution fusion | flops 4228096 | bytes 1075216 | tf_op jit(solution)/shard_map/dot_general | solution.py:99
  5.5 0.1 reshape.78
  5.6 0.8 %cosine_multiply_fusion = (f32[16,64]{1,0:T(8,128)S(1)}, f32[16,64]{1,0:T(8,128)S(1)}, f32[16,64]{1,0:T(8,128)S(1)}, f32[16,64]{1,0:T(8,128)S(1)}) fusion(f32[16,64]{1,0:T(8,128)} %param.24, f32[16,64]{1,0:T(8,128)} %param.23, f32[16]{0:T(128)S(1)} %exp.10), kind=kLoop, calls=%fused_computation.51 | loop fusion | flops 17408 | bytes 24640 | tf_op jit(solution)/shard_map/mul | solution.py:24
  6.4 1.2 %fusion.2 = f32[4,16,64]{2,0,1:T(4,128)S(1)} fusion(f32[16,64,16]{1,2,0:T(8,128)} %param.26, f32[16,64,16]{1,2,0:T(8,128)} %param.27, f32[16,64]{1,0:T(8,128)S(1)} %get-tuple-element.21, f32[16,64]{1,0:T(8,128)S(1)} %get-tuple-element.20, f32[4,16,64]{2,1,0:T(8,128)} %param.32, f32[4,16,64]{2,1,0:T(8,128)} %param.31, f32[16,64]{1,0:T(8,128)S(1)} %get-tuple-element.22, ...), kind=kOutput, calls=%fused_computation.6 | convolution fusion | flops 851968 | bytes 198656 | tf_op jit(solution)/shard_map/sgp,gnp->sgn/dot_general | solution.py:55
  7.6 1.2 %fusion.3 = f32[4,16,64]{2,0,1:T(4,128)S(1)} fusion(f32[16,64,16]{1,2,0:T(8,128)} %param.27, f32[16,64,16]{1,2,0:T(8,128)} %param.26, f32[16,64]{1,0:T(8,128)S(1)} %get-tuple-element.21, f32[16,64]{1,0:T(8,128)S(1)} %get-tuple-element.20, f32[4,16,64]{2,1,0:T(8,128)} %param.32, f32[4,16,64]{2,1,0:T(8,128)} %param.31, f32[16,64]{1,0:T(8,128)S(1)} %get-tuple-element.22, ...), kind=kOutput, calls=%fused_computation.8 | convolution fusion | flops 851968 | bytes 198656 | tf_op jit(solution)/shard_map/sgp,gnp->sgn/dot_general | solution.py:54
  8.8 0.1 fusion.45
  8.9 0.1 fusion.43
  9.0 0.7 %convert_element_type.80 = f32[2048]{0:T(1024)S(1)} convert(bf16[2048]{0:T(1024)(128)(2,1)} %param.34) | non-fusion elementwise | flops 2048 | bytes 12288 | tf_op jit(solution)/shard_map/convert_element_type | solution.py:15
  9.7 1.2 %fusion.60 = f32[16,4,16]{2,1,0:T(4,128)S(1)} fusion(f32[4,16,64]{2,0,1:T(4,128)S(1)} %fusion.3, f32[16,16,64]{2,1,0:T(8,128)} %param.28), kind=kOutput, calls=%fused_computation.84 | convolution fusion | flops 786432 | bytes 86016 | tf_op jit(solution)/shard_map/sgn,gpn->sgp/dot_general | solution.py:58
  10.9 1.2 %fusion.1 = f32[4,16,16]{2,0,1:T(4,128)S(1)} fusion(f32[16,4,16]{2,1,0:T(4,128)S(1)} %fusion.60, f32[4,16,64]{2,0,1:T(4,128)S(1)} %fusion.2, f32[16,16,64]{2,1,0:T(8,128)} %param.29), kind=kOutput, calls=%fused_computation.4 | convolution fusion | flops 787456 | bytes 90112 | tf_op jit(solution)/shard_map/sgn,gpn->sgp/dot_general | solution.py:58
  12.1 0.1 reshape.79
  12.2 0.0 copy-done
  12.2 0.9 %fusion.46 = f32[4,2048]{1,0:T(4,128)S(1)} fusion(bf16[256,2048]{1,0:T(8,128)(2,1)S(1)} %copy-done, f32[4,256]{1,0:T(4,128)S(1)} %reshape.79, bf16[4,256]{1,0:T(4,128)(2,1)S(1)} %convolution_convert_fusion.2, f32[256]{0:T(256)} %param.30), kind=kOutput, calls=%fused_computation.69 | convolution fusion | flops 4206592 | bytes 1088512 | tf_op jit(solution)/shard_map/dot_general | solution.py:115
  13.2 12.9 %psum.7 = f32[4,2048]{1,0:T(4,128)S(1)} all-reduce(f32[4,2048]{1,0:T(4,128)S(1)} %fusion.46), channel_id=1, replica_groups=mesh['ep'=8,'tp'=4] {'tp'}, use_global_device_ids=true, to_apply=%region_1.0 | all-reduce | flops 8192 | bytes 65536 | tf_op jit(solution)/shard_map/psum | solution.py:115
  26.1 0.9 %fusion.16 = (f32[4]{0:T(128)S(1)}, bf16[4,2048]{1,0:T(4,128)(2,1)S(1)}) fusion(f32[4,2048]{1,0:T(4,128)S(1)} %psum.7, bf16[4,2048]{1,0:T(4,128)(2,1)} %param.20), kind=kLoop, calls=%fused_computation.29 | loop fusion | flops 49148 | bytes 65552 | tf_op jit(solution)/shard_map/reduce_sum | solution.py:14
  26.9 0.8 %select_reduce_fusion.1 = (f32[4,8,2]{1,0,2:T(4,128)S(1)}, bf16[4,8,2]{1,0,2:T(4,128)(2,1)S(1)}) fusion(f32[4,2]{0,1:T(2,128)} %param.36, s32[4,2,8]{2,0,1:T(4,128)S(1)} %copy.75, pred[4,2,8]{2,0,1:T(4,128)(4,1)S(1)} %copy.76), kind=kLoop, calls=%fused_computation.45 | loop fusion | flops 640 | bytes 736 | tf_op jit(solution)/shard_map/reduce_sum | solution.py:72
  27.7 0.2 convolution_convert_fusion
  27.9 0.1 copy.77
  28.0 12.5 %all_to_all.10 = bf16[8,2,2048]{2,1,0:T(2,128)(2,1)S(1)} all-to-all(bf16[8,2,2048]{2,1,0:T(2,128)(2,1)S(1)} %copy.77), channel_id=1, replica_groups=mesh['ep'=8,'tp'=4] {'ep'}, dimensions={0} | all-to-all | bytes 131072 | tf_op jit(solution)/shard_map/all_to_all | solution.py:128
  40.5 0.0 copy-start.1
  40.6 0.0 slice-start
  40.6 4.7 %fusion.61 = f32[16,2048]{1,0:T(8,128)S(1)} fusion(bf16[16,2048]{1,0:T(8,128)(2,1)S(1)} %reshape.80, bf16[2048,2048]{1,0:T(8,128)(2,1)} %param.37), kind=kOutput, calls=%fused_computation.85 | convolution fusion | flops 134217728 | bytes 8585216 | tf_op jit(solution)/shard_map/dot_general | solution.py:132
  45.3 1.0 %copy-done.1 = bf16[2048,2048]{1,0:T(8,128)(2,1)S(1)} copy-done((bf16[2048,2048]{1,0:T(8,128)(2,1)S(1)}, bf16[2048,2048]{1,0:T(8,128)(2,1)}, u32[]{:S(2)}) %copy-start.1) | copy-done | bytes 8388632
  46.3 0.0 slice-start.1
  46.3 1.2 %fusion = bf16[16,2048]{1,0:T(8,128)(2,1)S(1)} fusion(bf16[16,2048]{1,0:T(8,128)(2,1)S(1)} %reshape.80, bf16[2048,2048]{1,0:T(8,128)(2,1)S(1)} %copy-done.1, f32[16,2048]{1,0:T(8,128)S(1)} %fusion.61), kind=kOutput, calls=%fused_computation.2 | convolution fusion | flops 134414336 | bytes 8650752 | tf_op jit(solution)/shard_map/dot_general | solution.py:133
  47.5 5.9 %all-gather = bf16[64,2048]{1,0:T(8,128)(2,1)S(1)} all-gather(bf16[16,2048]{1,0:T(8,128)(2,1)S(1)} %fusion), channel_id=2, replica_groups=mesh['ep'=8,'tp'=4] {'tp'}, dimensions={0}, use_global_device_ids=true | all-gather | bytes 327680 | tf_op jit(solution)/shard_map/all_gather | solution.py:137
  53.4 0.2 copy.78
  53.6 0.2 copy.82
  53.8 0.0 slice-done
  53.8 0.0 slice-done.1
  53.8 1.2 %convolution_convert_fusion.1 = bf16[16,512]{1,0:T(8,128)(2,1)S(1)} fusion(bf16[16,8192]{1,0:T(8,128)(2,1)S(1)} %bitcast.44, bf16[8192,512]{1,0:T(8,128)(2,1)S(1)} %bitcast.43), kind=kOutput, calls=%fused_computation.9 | convolution fusion | flops 134225920 | bytes 8667136 | tf_op jit(solution)/shard_map/dot_general | solution.py:136
  55.0 0.6 reshape.83
  55.6 3.3 %all-to-all-start.1 = ((bf16[8,2,512]{2,1,0:T(2,128)(2,1)}), bf16[8,2,512]{2,1,0:T(2,128)(2,1)S(1)}, u32[]{:S(2)}, u32[]{:S(2)}) async-start(bf16[8,2,512]{2,1,0:T(2,128)(2,1)} %reshape.83), calls=%async_computation.1 | async-start | bytes 32768 | tf_op jit(solution)/shard_map/all_to_all | solution.py:142
  59.0 0.6 copy.80
  59.6 0.6 copy.81
  60.2 5.3 %all-to-all-done.1 = bf16[8,2,512]{2,1,0:T(2,128)(2,1)S(1)} async-done(((bf16[8,2,512]{2,1,0:T(2,128)(2,1)}), bf16[8,2,512]{2,1,0:T(2,128)(2,1)S(1)}, u32[]{:S(2)}, u32[]{:S(2)}) %all-to-all-start.1) | async-done | bytes 16416 | tf_op jit(solution)/shard_map/all_to_all | solution.py:142
  65.5 0.8 %fusion.5 = bf16[4,512]{1,0:T(4,128)(2,1)} fusion(bf16[8,2,512]{2,1,0:T(2,128)(2,1)S(1)} %all-to-all-done.1, f32[4,8,2]{1,0,2:T(4,128)S(1)} %get-tuple-element.15, bf16[4,2048]{1,0:T(4,128)(2,1)S(1)} %get-tuple-element.18, s32[]{:T(128)S(6)} %select_n.13), kind=kOutput, calls=%fused_computation.12 | convolution fusion | flops 399360 | bytes 24836 | tf_op jit(solution)/shard_map/xcs,xcd->sd/dot_general | solution.py:147
  (8 shorter events, 0.1 us)
Async XLA Ops:
  0.6 11.6 %copy-start = (bf16[256,2048]{1,0:T(8,128)(2,1)S(1)}, bf16[256,2048]{1,0:T(8,128)(2,1)}, u32[]{:S(2)}) copy-start(bf16[256,2048]{1,0:T(8,128)(2,1)} %param.33) | copy-start | bytes 3145732
  40.5 5.8 %copy-start.1 = (bf16[2048,2048]{1,0:T(8,128)(2,1)S(1)}, bf16[2048,2048]{1,0:T(8,128)(2,1)}, u32[]{:S(2)}) copy-start(bf16[2048,2048]{1,0:T(8,128)(2,1)} %param.38) | copy-start | bytes 25165828
  40.6 13.2 %slice-start = ((s8[8388608]{0:T(1024)(128)(4,1)}), s8[4194304]{0:T(1024)(128)(4,1)S(1)}, s32[]{:S(2)}) async-start(s8[8388608]{0:T(1024)(128)(4,1)} %bitcast.42), calls=%async_computation.2 | async-start | bytes 8388608
  46.3 7.5 %slice-start.1 = ((s8[8388608]{0:T(1024)(128)(4,1)}), s8[4194304]{0:T(1024)(128)(4,1)S(1)}, s32[]{:S(2)}) async-start(s8[8388608]{0:T(1024)(128)(4,1)} %bitcast.42), calls=%async_computation.3 | async-start | bytes 8388608
  55.6 9.9 %all-to-all-start.1 = ((bf16[8,2,512]{2,1,0:T(2,128)(2,1)}), bf16[8,2,512]{2,1,0:T(2,128)(2,1)S(1)}, u32[]{:S(2)}, u32[]{:S(2)}) async-start(bf16[8,2,512]{2,1,0:T(2,128)(2,1)} %reshape.83), calls=%async_computation.1 | async-start | bytes 32768 | tf_op jit(solution)/shard_map/all_to_all | solution.py:142
